TPU v7x, 32 devices: a whole 2x2x4 slice. The times are simulated.
32 devices in a mesh: grp: 2 (over x), ep: 16 (over z, y, core).
Axes of the slice: x: 2, y: 2, z: 4, core: 2. Of those that a mesh axis runs over, the one named last changes fastest.
Arguments:
- tokens: bfloat16 [512, 2048], P(('grp', 'ep')), parts along dimension 0, may hold values from -6 to 6
- norm_gain: bfloat16 [2048], replicated, may hold values from 0.099609375 to 1.8984375
- query_weight: bfloat16 [2048, 1024], P(None, 'ep'), may hold values from -0.125 to 0.125
- key_weight: bfloat16 [2048, 256], replicated, may hold values from -0.25 to 0.25
- value_weight: bfloat16 [2048, 256], replicated, may hold values from -0.125 to 0.125
- out_weight: bfloat16 [1024, 2048], P(None, 'ep'), may hold values from -0.1875 to 0.1875
- head_gain: bfloat16 [128], replicated, may hold values from 0.099609375 to 1.8984375
- lambdas: float32 [8], replicated, may hold values from 0.3 to 0.8
- cache_keys: bfloat16 [512, 1024, 2, 128], P(('grp', 'ep')), parts along dimension 0, may hold values from -1000 to 1000
- cache_values: bfloat16 [512, 1024, 2, 128], P(('grp', 'ep')), parts along dimension 0, may hold values from -6 to 6
- lengths: int32 [512], P(('grp', 'ep')), parts along dimension 0, may hold values from 64 to 1024
- moe_gain: bfloat16 [2048], replicated, may hold values from 0.099609375 to 1.8984375
- gate_weight: bfloat16 [16, 2048, 1024], P('ep'), may hold values from -0.375 to 0.375
- up_weight: bfloat16 [16, 2048, 1024], P('ep'), may hold values from -0.375 to 0.375
- down_weight: bfloat16 [16, 1024, 2048], P('ep'), may hold values from -0.02734375 to 0.02734375
- routes: int32 [512, 4], P(('grp', 'ep')), parts along dimension 0, may hold values from 0 to 15, all different within a row; in each aligned block of 16 rows (0 to 15, 16 to 31, ...) at most 8 rows name the same one
- route_weights: float32 [512, 4], P(('grp', 'ep')), parts along dimension 0, may hold values from 0.2 to 1
Outputs:
- mixed: bfloat16 [512, 2048], P(('grp', 'ep')), parts along dimension 0
There are 2 independent parts, one for each index of `grp`. A program takes and returns all parts, laid end to end along the dimension named above; an argument that names none is the same for every part. Nothing has to cross between parts.
Inputs may be any that keep to these rules, and one draw needn't show every extreme that they name: `routes`: a token's 4 experts differ; the tokens of one device name each expert at most 8 times, and in every draw some expert is named exactly 8 times by one device's tokens.
All inputs are finite; a program needn't handle non-finite values.
Results may differ from a plain program's by a relative error of at most 0.034.
Values may be sent and summed in bfloat16 or wider, within the bound.
A program may use at most 128 MiB of HBM per device.

v0:
```python
import jax
import jax.numpy as jnp
from jax import lax
from jax.sharding import PartitionSpec as P

epsilon = 1e-06
masked_score = -1e30
clamp_limit = 7.0
swish_alpha = 1.702


def rms_scaled(values, gain):
    floats = values.astype(jnp.float32)
    return (
        floats
        * lax.rsqrt(jnp.mean(floats * floats, axis=-1, keepdims=True) + epsilon)
        * gain.astype(jnp.float32)
    )


def attention(queries, new_keys, new_values, cache_keys, cache_values, lengths, lambdas, head_gain):
    count = queries.shape[0]
    ctx_len = cache_keys.shape[1]
    kv_count = cache_keys.shape[2]
    head_dim = cache_keys.shape[3] // 2
    heads = lambdas.shape[0]
    group = heads // kv_count
    val_dim = cache_values.shape[3]
    query_grid = queries.reshape(count, kv_count, group, 2, head_dim)
    key_grid = cache_keys.reshape(count, ctx_len, kv_count, 2, head_dim)
    own_keys = new_keys.reshape(count, kv_count, 2, head_dim)
    inv_scale = head_dim ** (-0.5)
    scores = (
        jnp.einsum("bkgcd,bjkcd->bkgcj", query_grid, key_grid, preferred_element_type=jnp.float32)
        * inv_scale
    )
    own_score = (
        jnp.einsum("bkgcd,bkcd->bkgc", query_grid, own_keys, preferred_element_type=jnp.float32)
        * inv_scale
    )
    visible = jnp.arange(ctx_len, dtype=jnp.int32)[None, :] < lengths[:, None]
    scores = jnp.where(visible[:, None, None, None, :], scores, masked_score)
    highest = jnp.maximum(jnp.max(scores, axis=-1), own_score)
    expd = jnp.exp(scores - highest[..., None])
    own_exp = jnp.exp(own_score - highest)
    denominator = jnp.sum(expd, axis=-1) + own_exp
    probs = expd / denominator[..., None]
    own_prob = own_exp / denominator
    lambda_grid = lambdas.reshape(kv_count, group)[None, :, :]
    weights = (probs[:, :, :, 0] - lambda_grid[..., None] * probs[:, :, :, 1]).astype(jnp.bfloat16)
    own_weight = (own_prob[..., 0] - lambda_grid * own_prob[..., 1]).astype(jnp.bfloat16)
    attended = jnp.einsum(
        "bkgj,bjkv->bkgv", weights, cache_values, preferred_element_type=jnp.float32
    )
    own_vals = new_values.reshape(count, kv_count, val_dim).astype(jnp.float32)
    attended = attended + own_weight.astype(jnp.float32)[..., None] * own_vals[:, :, None, :]
    return rms_scaled(attended, head_gain).reshape(count, heads * val_dim).astype(jnp.bfloat16)


def expert_mlp(inputs, gate_w, up_w, down_w):
    gate = jnp.dot(inputs, gate_w, preferred_element_type=jnp.float32)
    upper = jnp.dot(inputs, up_w, preferred_element_type=jnp.float32)
    gate = jnp.minimum(gate, clamp_limit)
    upper = jnp.clip(upper, -clamp_limit, clamp_limit)
    act = ((upper + 1.0) * gate * jax.nn.sigmoid(swish_alpha * gate)).astype(jnp.bfloat16)
    return jnp.dot(act, down_w, preferred_element_type=jnp.float32).astype(jnp.bfloat16)


def local(
    tokens,
    norm_gain,
    query_weight,
    key_weight,
    value_weight,
    out_weight,
    head_gain,
    lambdas,
    cache_keys,
    cache_values,
    lengths,
    moe_gain,
    gate_weight,
    up_weight,
    down_weight,
    routes,
    route_weights,
):
    count = tokens.shape[0]
    width = tokens.shape[1]
    topk = routes.shape[1]
    normed = rms_scaled(tokens, norm_gain).astype(jnp.bfloat16)
    new_keys = jnp.dot(normed, key_weight, preferred_element_type=jnp.float32).astype(jnp.bfloat16)
    new_values = jnp.dot(normed, value_weight, preferred_element_type=jnp.float32).astype(
        jnp.bfloat16
    )
    queries = jnp.dot(
        normed,
        lax.all_gather(query_weight, "ep", axis=1, tiled=True),
        preferred_element_type=jnp.float32,
    ).astype(jnp.bfloat16)
    head_out = attention(
        queries, new_keys, new_values, cache_keys, cache_values, lengths, lambdas, head_gain
    )
    attn_out = jnp.dot(
        head_out,
        lax.all_gather(out_weight, "ep", axis=1, tiled=True),
        preferred_element_type=jnp.float32,
    ).astype(jnp.bfloat16)
    residual = (tokens.astype(jnp.float32) + attn_out.astype(jnp.float32)).astype(jnp.bfloat16)
    moe_in = rms_scaled(residual, moe_gain).astype(jnp.bfloat16)
    experts = lax.axis_size("ep")
    capacity = min(count, max(2, 2 * count * topk // experts))
    onehot = (routes.reshape(-1)[:, None] == jnp.arange(experts, dtype=jnp.int32)[None, :]).astype(
        jnp.int32
    )
    earlier_all = jnp.cumsum(onehot, axis=0) - onehot
    ranks = jnp.sum(earlier_all * onehot, axis=1).reshape(count, topk)
    slot_id = routes * capacity + ranks
    slot_range = jnp.arange(experts * capacity, dtype=jnp.int32)
    dispatch = jnp.any(slot_id[None, :, :] == slot_range[:, None, None], axis=2).astype(
        jnp.bfloat16
    )
    outgoing = jnp.dot(dispatch, moe_in, preferred_element_type=jnp.float32).astype(jnp.bfloat16)
    outgoing = outgoing.reshape(experts, capacity, width)
    received = lax.all_to_all(outgoing, "ep", split_axis=0, concat_axis=0, tiled=True)
    flat_rows = received.reshape(-1, width)
    results = expert_mlp(flat_rows, gate_weight[0], up_weight[0], down_weight[0]).reshape(
        received.shape
    )
    returned = lax.all_to_all(results, "ep", split_axis=0, concat_axis=0, tiled=True)
    picked = returned.reshape(-1, width)[slot_id].astype(jnp.float32)
    moe_sum = jnp.sum(route_weights[:, :, None] * picked, axis=1)
    return (residual.astype(jnp.float32) + moe_sum).astype(jnp.bfloat16)


def solution(mesh):
    placed = (
        P(("grp", "ep"), None),
        P(),
        P(None, "ep"),
        P(),
        P(),
        P(None, "ep"),
        P(),
        P(),
        P(("grp", "ep"), None, None, None),
        P(("grp", "ep"), None, None, None),
        P(("grp", "ep")),
        P(),
        P("ep", None, None),
        P("ep", None, None),
        P("ep", None, None),
        P(("grp", "ep"), None),
        P(("grp", "ep"), None),
    )
    return jax.shard_map(
        local, mesh=mesh, in_specs=placed, out_specs=P(("grp", "ep"), None), check_vma=False
    )
```

profile of v0, /device:TPU:0, one launch (start us, length us, event | category | flops | bytes accessed | tf_op | source)
XLA Modules:
  0.0 169.9 jit_solution(1162133540480479618)
XLA Ops:
  6.5 0.0 copy-start
  6.5 0.7 all-gather.3.cloned.1.call-update
  7.3 0.0 all-gather.5.cloned.1.call-start
  7.3 0.7 all-gather.5.cloned.1.call-update
  8.0 0.7 convert_element_type.86
  8.7 1.0 fusion.64
  9.7 1.1 convolution_convert_fusion.4
  10.8 0.1 reshape.109
  10.9 0.0 copy-start.8
  10.9 0.0 copy-start.2
  10.9 0.0 copy-start.3
  10.9 0.0 copy-start.9
  10.9 0.0 copy-start.5
  11.0 0.0 copy-start.4
  11.0 0.0 copy-start.7
  11.0 21.3 %copy.71 = bf16[16,1024,2,128]{1,3,2,0:T(8,128)(2,1)} copy(bf16[16,1024,2,128]{3,2,1,0:T(2,128)(2,1)} %param.25) | data formatting | bytes 16777216 | tf_op args[8]
  32.3 0.1 mul.149
  32.4 0.0 copy-done.3
  32.4 0.3 fusion.42
  32.7 0.1 copy.83
  32.8 0.1 eq.28
  32.9 0.1 fusion.72
  33.0 0.1 reduce_window_sum.11
  33.1 0.2 select_reduce_fusion
  33.3 0.1 reshape.88
  33.3 0.1 copy.85
  33.4 0.0 copy-done.4
  33.4 0.1 fusion.73
  33.5 0.0 copy-done.7
  33.5 0.1 iota_compare_fusion
  33.6 29.0 %all-gather.3.cloned.1.call-done = bf16[2048,1024]{0,1:T(8,128)(2,1)} async-done(((bf16[2048,64]{0,1:T(8,128)(2,1)}), bf16[2048,1024]{0,1:T(8,128)(2,1)}) %all-gather.3.cloned.1.call-update) | async-done | bytes 4194320 | tf_op jit(solution)/shard_map/all_gather | solution.py:98
  62.6 3.4 %convolution_convert_fusion.2 = bf16[16,1024]{1,0:T(8,128)(2,1)S(1)} fusion(bf16[2048,1024]{0,1:T(8,128)(2,1)} %all-gather.3.cloned.1.call-done, bf16[16,2048]{1,0:T(8,128)(2,1)S(1)} %copy-done.2, f32[2048]{0:T(1024)S(1)} %convert_element_type.86, f32[16]{0:T(128)S(1)} %add_rsqrt_fusion.2), kind=kOutput, calls=%fused_computation.28 | convolution fusion | flops 67256320 | bytes 4300864 | tf_op jit(solution)/shard_map/dot_general | solution.py:96
  66.0 0.1 reshape.85
  66.1 0.2 fusion.69
  66.3 0.1 copy.87
  66.4 4.7 %fusion.88 = (f32[16,2,4,2]{2,3,1,0:T(2,128)S(1)}, f32[16,2,4,2,1024]{4,2,3,1,0:T(4,128)S(1)}) fusion(bf16[16,1024,2,2,64]{1,4,3,2,0:T(8,128)(2,1)} %bitcast.105, bf16[16,2,4,2,64]{4,3,2,1,0:T(2,128)(2,1)S(1)} %reshape.85, pred[16,1024]{1,0:T(8,128)(4,1)S(1)} %iota_compare_fusion), kind=kOutput, calls=%fused_computation.95 | convolution fusion | flops 34340608 | bytes 9487360 | tf_op jit(solution)/shard_map/bkgcd,bjkcd->bkgcj/dot_general | solution.py:34
  71.2 0.1 copy.73
  71.3 0.1 copy.74
  71.4 0.5 fusion.44
  71.9 0.1 copy.75
  72.1 0.1 copy.76
  72.2 0.1 fusion.78
  72.2 0.1 copy.79
  72.3 0.5 fusion.43
  72.8 4.9 %multiply_reduce_fusion.2 = (f32[16,2,4]{2,1,0:T(2,128)S(1)}, f32[16,2,4,128]{3,2,1,0:T(4,128)S(1)}) fusion(f32[16,2,128]{2,1,0:T(2,128)S(1)} %reshape.94, f32[16,2,4]{2,1,0:T(2,128)S(1)} %copy.79, bf16[16,1024,2,128]{3,2,1,0:T(2,128)(2,1)} %param.26, f32[16,2,4,2,1024]{4,2,3,1,0:T(4,128)S(1)} %fusion.43, f32[2,4]{1,0:T(2,128)S(1)} %mul.149), kind=kOutput, calls=%fused_computation.64 | convolution fusion | flops 34013056 | bytes 9520160 | tf_op jit(solution)/shard_map/bkgj,bjkv->bkgv/dot_general | solution.py:52
  77.8 0.1 copy.80
  77.9 0.1 copy.81
  78.0 0.1 multiply_convert_fusion.2
  78.1 37.6 %all-gather.5.cloned.1.call-done = bf16[1024,2048]{1,0:T(8,128)(2,1)} async-done(((bf16[1024,128]{1,0:T(8,128)(2,1)}), bf16[1024,2048]{1,0:T(8,128)(2,1)}) %all-gather.5.cloned.1.call-update) | async-done | bytes 4194320 | tf_op jit(solution)/shard_map/all_gather | solution.py:106
  115.7 3.1 %multiply_reduce_fusion.1 = (f32[16]{0:T(128)S(1)}, f32[16,2048]{1,0:T(8,128)S(1)}) fusion(bf16[16,1024]{1,0:T(8,128)(2,1)S(1)} %convert_element_type.97, bf16[1024,2048]{1,0:T(8,128)(2,1)} %all-gather.5.cloned.1.call-done, bf16[16,2048]{1,0:T(8,128)(2,1)S(1)} %copy-done.2), kind=kOutput, calls=%fused_computation.60 | convolution fusion | flops 67370992 | bytes 4423744 | tf_op jit(solution)/shard_map/dot_general | solution.py:104
  118.9 0.3 fusion.14
  119.2 17.0 %all_to_all.10 = bf16[16,8,2048]{2,1,0:T(8,128)(2,1)S(1)} all-to-all(bf16[16,8,2048]{2,1,0:T(8,128)(2,1)S(1)} %fusion.14), channel_id=1, replica_groups=mesh['grp'=2,'ep'=16] {'ep'}, dimensions={0} | all-to-all | bytes 1048576 | tf_op jit(solution)/shard_map/all_to_all | solution.py:125
  136.2 0.0 copy-done.1
  136.2 0.7 fusion.24
  136.9 0.0 copy-start.6
  136.9 5.7 %fusion.11 = bf16[16,8,2048]{2,1,0:T(8,128)(2,1)} fusion(bf16[1,1024,2048]{2,1,0:T(8,128)(2,1)} %param.31, f32[128,1024]{1,0:T(8,128)S(1)} %fusion.24, bf16[1,2048,1024]{2,1,0:T(8,128)(2,1)} %param.30, bf16[16,8,2048]{2,1,0:T(8,128)(2,1)S(1)} %all_to_all.10), kind=kOutput, calls=%fused_computation.11 | convolution fusion | flops 1075183616 | bytes 9961472 | tf_op jit(solution)/shard_map/dot_general | solution.py:66
  142.6 4.2 %all-to-all-start.1 = ((bf16[16,8,2048]{2,1,0:T(8,128)(2,1)}), bf16[16,8,2048]{2,1,0:T(8,128)(2,1)S(1)}, u32[]{:S(2)}, u32[]{:S(2)}) async-start(bf16[16,8,2048]{2,1,0:T(8,128)(2,1)} %fusion.11), calls=%async_computation.1 | async-start | bytes 1048576 | tf_op jit(solution)/shard_map/all_to_all | solution.py:130
  146.8 0.1 reshape.97
  146.9 0.1 copy.82
  147.0 14.1 %all-to-all-done.1 = bf16[16,8,2048]{2,1,0:T(8,128)(2,1)S(1)} async-done(((bf16[16,8,2048]{2,1,0:T(8,128)(2,1)}), bf16[16,8,2048]{2,1,0:T(8,128)(2,1)S(1)}, u32[]{:S(2)}, u32[]{:S(2)}) %all-to-all-start.1) | async-done | bytes 524320 | tf_op jit(solution)/shard_map/all_to_all | solution.py:130
  161.1 0.7 gather_fusion
  161.8 0.2 reshape.105
  162.0 0.4 multiply_reduce_fusion
  162.4 0.6 add_convert_fusion
  (19 shorter events, 0.1 us)
Async XLA Ops:
  6.5 3.1 %copy-start = (bf16[2048,256]{1,0:T(8,128)(2,1)S(1)}, bf16[2048,256]{1,0:T(8,128)(2,1)}, u32[]{:S(2)}) copy-start(bf16[2048,256]{1,0:T(8,128)(2,1)} %param.20) | copy-start | bytes 3145732
  6.5 56.1 %all-gather.3.cloned.1.call-start = ((), (), s32[]{:S(2)}) async-start(), calls=%async_computation.2 | async-start | bytes 4456448 | tf_op jit(solution)/shard_map/all_gather | solution.py:98
  7.3 108.5 %all-gather.5.cloned.1.call-start = ((), (), s32[]{:S(2)}) async-start(), calls=%async_computation.3 | async-start | bytes 4456448 | tf_op jit(solution)/shard_map/all_gather | solution.py:106
  10.9 21.4 %copy-start.8 = (f32[8]{0:T(128)S(1)}, f32[8]{0:T(128)}, u32[]{:S(2)}) copy-start(f32[8]{0:T(128)} %param.24) | copy-start | bytes 100
  10.9 21.5 %copy-start.2 = (bf16[16,2048]{1,0:T(8,128)(2,1)S(1)}, bf16[16,2048]{1,0:T(8,128)(2,1)}, u32[]{:S(2)}) copy-start(bf16[16,2048]{1,0:T(8,128)(2,1)} %param.17) | copy-start | bytes 196612
  10.9 21.4 %copy-start.3 = (bf16[2048,256]{1,0:T(8,128)(2,1)S(1)}, bf16[2048,256]{1,0:T(8,128)(2,1)}, u32[]{:S(2)}) copy-start(bf16[2048,256]{1,0:T(8,128)(2,1)} %param.21) | copy-start | bytes 3145732
  10.9 21.7 %copy-start.9 = (bf16[128]{0:T(256)(128)(2,1)S(1)}, bf16[128]{0:T(256)(128)(2,1)}, u32[]{:S(2)}) copy-start(bf16[128]{0:T(256)(128)(2,1)} %param.23) | copy-start | bytes 772
  10.9 21.8 %copy-start.5 = (s32[16,4]{0,1:T(4,128)S(1)}, s32[16,4]{0,1:T(4,128)}, u32[]{:S(2)}) copy-start(s32[16,4]{0,1:T(4,128)} %param.32) | copy-start | bytes 772
  11.0 22.5 %copy-start.4 = (bf16[2048]{0:T(1024)(128)(2,1)S(1)}, bf16[2048]{0:T(1024)(128)(2,1)}, u32[]{:S(2)}) copy-start(bf16[2048]{0:T(1024)(128)(2,1)} %param.28) | copy-start | bytes 12292
  11.0 22.6 %copy-start.7 = (s32[16]{0:T(128)S(1)}, s32[16]{0:T(128)}, u32[]{:S(2)}) copy-start(s32[16]{0:T(128)} %param.27) | copy-start | bytes 196
  115.7 20.4 %copy-start.1 = (bf16[1,2048,1024]{2,1,0:T(8,128)(2,1)S(1)}, bf16[1,2048,1024]{2,1,0:T(8,128)(2,1)}, u32[]{:S(2)}) copy-start(bf16[1,2048,1024]{2,1,0:T(8,128)(2,1)} %param.29) | copy-start | bytes 12582916
  136.9 10.0 %copy-start.6 = (f32[16,4]{0,1:T(4,128)S(1)}, f32[16,4]{0,1:T(4,128)}, u32[]{:S(2)}) copy-start(f32[16,4]{0,1:T(4,128)} %param.33) | copy-start | bytes 772
  142.6 18.4 %all-to-all-start.1 = ((bf16[16,8,2048]{2,1,0:T(8,128)(2,1)}), bf16[16,8,2048]{2,1,0:T(8,128)(2,1)S(1)}, u32[]{:S(2)}, u32[]{:S(2)}) async-start(bf16[16,8,2048]{2,1,0:T(8,128)(2,1)} %fusion.11), calls=%async_computation.1 | async-start | bytes 1048576 | tf_op jit(solution)/shard_map/all_to_all | solution.py:130
Sparse Core Ops, SparseCore 0:
  9.5 53.0 all-gather.2
  64.8 50.9 all-gather.4
where the time goes:
time: 171 us; the launch traced here: 170 us
  waiting for transfers between devices  82.1 us (48%)
  matrix products  24.5 us (14%)
  local copies, waits for them, and re-layouts  23.9 us (14%)
  blocking collectives  17 us (10%)
  between operations  13.6 us (8%)
  other arithmetic  4.52 us (3%)
  starting transfers between devices  4.2 us (2%)
    all_gather x1, waiting for transfers between devices, local(): lax.all_gather(out_weight, 'ep', axis=1, tiled=True)  37.6 us
    all_gather x1, waiting for transfers between devices, local(): lax.all_gather(query_weight, 'ep', axis=1, tiled=True)  29 us
    unnamed x23, local copies, waits for them, and re-layouts  21.5 us
    all_to_all x1, blocking collectives, local(): lax.all_to_all(outgoing, 'ep', split_axis=0, concat_axis=0, tiled=True)  17 us
    all_to_all x1, waiting for transfers between devices, local(): lax.all_to_all(results, 'ep', split_axis=0, concat_axis=0, tiled=True)  14.1 us
    dot_general x1, matrix products, expert_mlp(): jnp.dot(act, down_w, preferred_element_type=jnp.float32)  5.7 us
    dot_general x1, matrix products, attention(): jnp.einsum('bkgj,bjkv->bkgv', weights, cache_values, preferred_element_ty...  4.92 us
    dot_general x1, matrix products, attention(): jnp.einsum('bkgcd,bjkcd->bkgcj', query_grid, key_grid, preferred_element_...  4.71 us
  transfers between devices with their start and end apart: 3, of which 3 were waited for; matrix products, arithmetic and copies ran while one was open for 24% of the time, Pallas kernels for 0%

commit v1 on v0

v1 whole, which is shorter than its diff:
```python
import functools

import jax
import jax.numpy as jnp
from jax import lax
from jax.experimental import pallas as pl
from jax.experimental.pallas import tpu as pltpu
from jax.sharding import PartitionSpec as P

epsilon = 1e-06
masked_score = -1e30
clamp_limit = 7.0
swish_alpha = 1.702
f32 = jnp.float32
bf16 = jnp.bfloat16


def rms_scaled(values, gain):
    floats = values.astype(f32)
    scale = lax.rsqrt(jnp.mean(floats * floats, axis=-1, keepdims=True) + epsilon)
    return floats * scale * gain.astype(f32)


def layer_kernel(
    n,
    tokens_ref,
    norm_gain_ref,
    head_gain_ref,
    moe_gain_ref,
    lambdas_ref,
    lengths_ref,
    shares_ref,
    wq_hbm,
    wk_hbm,
    wv_hbm,
    wo_hbm,
    keys_hbm,
    values_hbm,
    gate_hbm,
    up_hbm,
    down_hbm,
    out_ref,
    wq,
    wk,
    wv,
    wo,
    keys,
    values,
    gate_w,
    up_w,
    down_w,
    normed_all,
    heads_all,
    moe_all,
    q_out,
    q_in,
    ao_out,
    ao_in,
    shares_in,
    q_grid,
    own_k,
    own_v,
    ho_grid,
    residual,
    act,
    y_out,
    rs_sib,
    rs_y_send,
    rs_y,
    rs_z_send,
    rs_z,
    w_sem,
    k_sem,
    v_sem,
    send_sem,
    recv_sem,
):
    me = lax.axis_index("ep")
    A = n // 4
    a, b, c = me // 4, (me // 2) % 2, me % 2
    count, width = tokens_ref.shape
    heads = lambdas_ref.shape[0]
    ctx2, lanes = keys.shape[1], keys.shape[2]
    kv_count = wk.shape[1] // lanes
    group = heads // kv_count
    dh = lanes // 2
    val = values.shape[2]

    def idx(i, j, k):
        return (i * 2 + j) * 2 + k

    def fwd(d):
        return lax.rem(a + d, A)

    def back(d):
        return lax.rem(a - d + A, A)

    ydev, sdev = idx(a, 1 - b, c), idx(a, b, 1 - c)
    sent = []

    def remote(src, dst, k, j, dev):
        return pltpu.make_async_remote_copy(
            src_ref=src,
            dst_ref=dst,
            send_sem=send_sem.at[k, j],
            recv_sem=recv_sem.at[k, j],
            device_id={"ep": dev},
            device_id_type=pl.DeviceIdType.MESH,
        )

    def start(copy):
        copy.start()
        sent.append(copy)

    loads = [
        pltpu.make_async_copy(src, dst, w_sem.at[i])
        for i, (src, dst) in enumerate(
            [
                (wq_hbm, wq),
                (wk_hbm, wk),
                (wv_hbm, wv),
                (wo_hbm, wo),
                (gate_hbm.at[0], gate_w),
                (up_hbm.at[0], up_w),
                (down_hbm.at[0], down_w),
            ]
        )
    ]

    def key_load(s):
        return pltpu.make_async_copy(keys_hbm.at[s], keys.at[s], k_sem.at[s])

    def value_load(s):
        return pltpu.make_async_copy(values_hbm.at[s], values.at[s], v_sem.at[s])

    barrier = pltpu.get_barrier_semaphore()

    def greet(d, carry):
        pl.semaphore_signal(
            barrier,
            inc=1,
            device_id={"ep": lax.rem(me + d, n)},
            device_id_type=pl.DeviceIdType.MESH,
        )
        return carry

    lax.fori_loop(1, n, greet, 0)
    for i in range(4):
        loads[i].start()

    def cache_load(s, carry):
        key_load(s).start()
        value_load(s).start()
        return carry

    lax.fori_loop(0, count, cache_load, 0)
    for i in range(4, 7):
        loads[i].start()

    normed_all[me] = rms_scaled(tokens_ref[...], norm_gain_ref[...]).astype(bf16)
    pl.semaphore_wait(barrier, n - 1)

    def gather(buf, k):
        def cp(slot, j, dev):
            return remote(buf.at[slot], buf.at[slot], k, j, dev)

        for d in range(1, A):
            start(cp(me, d - 1, idx(fwd(d), b, c)))
        start(cp(me, A - 1, ydev))
        start(cp(me, 2 * A - 1, sdev))
        for d in range(1, A):
            slot = idx(back(d), b, c)
            cp(slot, d - 1, me).wait_recv()
            start(cp(slot, A - 1 + d, ydev))
            start(cp(slot, 2 * A - 1 + d, sdev))
        for d in range(A):
            slot = idx(back(d), 1 - b, c)
            cp(slot, A - 1 + d, me).wait_recv()
            start(cp(slot, 3 * A - 1 + d, sdev))
        for d in range(A):
            cp(idx(back(d), b, 1 - c), 2 * A - 1 + d, me).wait_recv()
        for d in range(A):
            cp(idx(back(d), 1 - b, 1 - c), 3 * A - 1 + d, me).wait_recv()

    def exchange_start(src, dst, k):
        def body(d, carry):
            peer = lax.rem(me + d, n)
            remote(src.at[peer], dst.at[me], k, d - 1, peer).start()
            return carry

        lax.fori_loop(1, n, body, 0)

    def exchange_wait(src, dst, k):
        def body(d, carry):
            peer = lax.rem(me - d + n, n)
            remote(src.at[peer], dst.at[peer], k, d - 1, peer).wait_recv()
            return carry

        lax.fori_loop(1, n, body, 0)

    def exchange_drain(src, dst, k):
        def body(d, carry):
            peer = lax.rem(me + d, n)
            remote(src.at[peer], dst.at[me], k, d - 1, peer).wait_send()
            return carry

        lax.fori_loop(1, n, body, 0)

    def spread(block):
        w = block.shape[1]
        if w == lanes:
            return block.astype(bf16)
        row = lax.broadcasted_iota(jnp.int32, (w, lanes), 0)
        col = lax.broadcasted_iota(jnp.int32, (w, lanes), 1)
        pick = (row + lax.rem(me * w, lanes) == col).astype(f32).astype(bf16)
        return jnp.dot(block.astype(bf16), pick, preferred_element_type=f32).astype(bf16)

    gather(normed_all, 0)
    exchange_start(shares_ref, shares_in, 6)
    shares_in[me] = shares_ref[me]
    loads[0].wait()
    q = jnp.dot(
        normed_all[...].reshape(n * count, width), wq[...], preferred_element_type=f32
    )
    q_out[...] = spread(q).reshape(n, count, lanes)
    exchange_start(q_out, q_in, 3)
    q_in[me] = q_out[me]
    loads[1].wait()
    loads[2].wait()
    mine = normed_all[me]
    own_k[:, 0, :] = jnp.dot(mine, wk[...], preferred_element_type=f32).astype(bf16).astype(f32)
    own_v[:, 0, :] = jnp.dot(mine, wv[...], preferred_element_type=f32).astype(bf16).astype(f32)
    exchange_wait(q_out, q_in, 3)
    parts = n // (2 * heads)
    for h in range(heads):
        for m in range(2):
            first = (2 * h + m) * parts
            total = q_in[first].astype(f32)
            for i in range(1, parts):
                total = total + q_in[first + i].astype(f32)
            q_grid[:, m * heads + h, :] = total

    inv_scale = dh ** (-0.5)
    rows = 2 * heads
    kv_of = lax.rem(lax.broadcasted_iota(jnp.int32, (rows, ctx2), 0), heads) // group
    column = lax.broadcasted_iota(jnp.int32, (rows, ctx2), 1)
    lam = lambdas_ref[...]
    row_kv = lax.rem(lax.broadcasted_iota(jnp.int32, (rows, lanes), 0), heads) // group
    head_gain = head_gain_ref[...].astype(f32)

    def attend(s, carry):
        key_load(s).wait()
        value_load(s).wait()
        qs = q_grid[s]
        own_key = jnp.zeros((rows, lanes), f32)
        own_val = jnp.zeros((heads, val), f32)
        for kv in range(kv_count):
            own_key = jnp.where(row_kv == kv, own_k[s, :, kv * lanes : (kv + 1) * lanes], own_key)
            own_val = jnp.where(
                row_kv[:heads] == kv, own_v[s, :, kv * val : (kv + 1) * val], own_val
            )
        own_score = jnp.sum(qs * own_key, axis=1, keepdims=True) * inv_scale
        scores = (
            lax.dot_general(
                qs.astype(bf16),
                keys[s],
                (((1,), (1,)), ((), ())),
                preferred_element_type=f32,
            )
            * inv_scale
        )
        limit = lengths_ref[s] * kv_count
        visible = (lax.rem(column, kv_count) == kv_of) & (column < limit)
        scores = jnp.where(visible, scores, masked_score)
        highest = jnp.maximum(jnp.max(scores, axis=1, keepdims=True), own_score)
        expd = jnp.exp(scores - highest)
        own_exp = jnp.exp(own_score - highest)
        inv = 1.0 / (jnp.sum(expd, axis=1, keepdims=True) + own_exp)
        probs = expd * inv
        own_prob = own_exp * inv
        weights = (probs[:heads] - lam * probs[heads:]).astype(bf16)
        own_weight = (own_prob[:heads] - lam * own_prob[heads:]).astype(bf16).astype(f32)
        attended = jnp.dot(weights, values[s], preferred_element_type=f32)
        attended = attended + own_weight * own_val
        ho_grid[s] = rms_scaled(attended, head_gain)
        return carry

    lax.fori_loop(0, count, attend, 0)
    for h in range(heads):
        heads_all[me, :, h * val : (h + 1) * val] = ho_grid[:, h, :].astype(bf16)

    gather(heads_all, 1)
    loads[3].wait()
    ao = jnp.dot(
        heads_all[...].reshape(n * count, heads * val), wo[...], preferred_element_type=f32
    )
    ao_out[...] = spread(ao).reshape(n, count, lanes)
    exchange_start(ao_out, ao_in, 4)
    ao_in[me] = ao_out[me]
    exchange_wait(ao_out, ao_in, 4)
    per = n * lanes // width
    for t in range(width // lanes):
        total = ao_in[t * per].astype(f32)
        for i in range(1, per):
            total = total + ao_in[t * per + i].astype(f32)
        cols = slice(t * lanes, (t + 1) * lanes)
        residual[:, cols] = (tokens_ref[:, cols].astype(f32) + total).astype(bf16).astype(f32)
    moe_all[me] = rms_scaled(residual[...], moe_gain_ref[...]).astype(bf16)

    gather(moe_all, 2)
    for i in range(4, 7):
        loads[i].wait()
    total_rows = n * count
    ff = gate_w.shape[1]
    tile = 256

    def hidden(i, carry):
        cols = pl.ds(pl.multiple_of(i * tile, tile), tile)
        x = moe_all[...].reshape(total_rows, width)
        gate = jnp.dot(x, gate_w[:, cols], preferred_element_type=f32)
        upper = jnp.dot(x, up_w[:, cols], preferred_element_type=f32)
        gate = jnp.minimum(gate, clamp_limit)
        upper = jnp.clip(upper, -clamp_limit, clamp_limit)
        act[:, cols] = ((upper + 1.0) * gate * jax.nn.sigmoid(swish_alpha * gate)).astype(bf16)
        return carry

    lax.fori_loop(0, ff // tile, hidden, 0)
    exchange_wait(shares_ref, shares_in, 6)
    diagonal = lax.broadcasted_iota(jnp.int32, (n, count, lanes), 1) == lax.broadcasted_iota(
        jnp.int32, (n, count, lanes), 2
    )
    share = jnp.sum(jnp.where(diagonal, shares_in[...], 0.0), axis=2, keepdims=True)
    share = share.reshape(total_rows, 1)

    def project(i, carry):
        cols = pl.ds(pl.multiple_of(i * tile, tile), tile)
        y = jnp.dot(act[...], down_w[:, cols], preferred_element_type=f32)
        y_out[:, :, cols] = (y * share).astype(bf16).reshape(n, count, tile)
        return carry

    lax.fori_loop(0, width // tile, project, 0)

    order = list(range(1, A)) + [0]

    def sib(d, j):
        return remote(
            y_out.at[idx(fwd(d), lax.rem(b + j, 2), 1 - c)],
            rs_sib.at[fwd(d) * 2 + lax.rem(b + j, 2)],
            5,
            2 * A - 1 + j * A + d,
            sdev,
        )

    for j in (1, 0):
        for d in order:
            start(sib(d, j))
    ycopies, zcopies = {}, {}
    for d in order:
        sib(d, 1).wait_recv()
        dest = fwd(d)
        rs_y_send[d] = (
            y_out[idx(dest, 1 - b, c)].astype(f32) + rs_sib[dest * 2 + 1 - b].astype(f32)
        ).astype(bf16)
        ycopies[d] = remote(rs_y_send.at[d], rs_y.at[d], 5, A - 1 + d, ydev)
        start(ycopies[d])
    total = residual[...]
    for d in order:
        sib(d, 0).wait_recv()
        ycopies[d].wait_recv()
        dest = fwd(d)
        part = (
            y_out[idx(dest, b, c)].astype(f32)
            + rs_sib[dest * 2 + b].astype(f32)
            + rs_y[d].astype(f32)
        )
        if d:
            rs_z_send[d - 1] = part.astype(bf16)
            zcopies[d] = remote(
                rs_z_send.at[d - 1], rs_z.at[d - 1], 5, d - 1, idx(dest, b, c)
            )
            start(zcopies[d])
        else:
            total = total + part
    for d in range(1, A):
        zcopies[d].wait_recv()
        total = total + rs_z[d - 1].astype(f32)
    out_ref[...] = total.astype(bf16)
    for copy in sent:
        copy.wait_send()
    exchange_drain(q_out, q_in, 3)
    exchange_drain(ao_out, ao_in, 4)
    exchange_drain(shares_ref, shares_in, 6)


def local(
    n,
    tokens,
    norm_gain,
    query_weight,
    key_weight,
    value_weight,
    out_weight,
    head_gain,
    lambdas,
    cache_keys,
    cache_values,
    lengths,
    moe_gain,
    gate_weight,
    up_weight,
    down_weight,
    routes,
    route_weights,
):
    count, width = tokens.shape
    heads = lambdas.shape[0]
    ctx, kv_count, lanes = cache_keys.shape[1:]
    val = cache_values.shape[3]
    ctx2 = ctx * kv_count
    ff = gate_weight.shape[2]
    A = n // 4
    experts = jnp.arange(n, dtype=jnp.int32)[:, None, None]
    shares = jnp.sum(jnp.where(routes[None] == experts, route_weights[None], 0.0), axis=2)
    shares = jnp.pad(shares, ((0, 0), (0, lanes - count)))[:, None, :]
    vmem = pl.BlockSpec(memory_space=pltpu.VMEM)
    smem = pl.BlockSpec(memory_space=pltpu.SMEM)
    hbm = pl.BlockSpec(memory_space=pl.ANY)
    scratch = [
        (query_weight.shape, bf16),
        (key_weight.shape, bf16),
        (value_weight.shape, bf16),
        (out_weight.shape, bf16),
        ((count, ctx2, lanes), bf16),
        ((count, ctx2, val), bf16),
        ((width, ff), bf16),
        ((width, ff), bf16),
        ((ff, width), bf16),
        ((n, count, width), bf16),
        ((n, count, heads * val), bf16),
        ((n, count, width), bf16),
        ((n, count, lanes), bf16),
        ((n, count, lanes), bf16),
        ((n, count, lanes), bf16),
        ((n, count, lanes), bf16),
        ((n, 1, lanes), f32),
        ((count, 2 * heads, lanes), f32),
        ((count, 1, kv_count * lanes), f32),
        ((count, 1, kv_count * val), f32),
        ((count, heads, val), f32),
        ((count, width), f32),
        ((n * count, ff), bf16),
        ((n, count, width), bf16),
        ((2 * A, count, width), bf16),
        ((A, count, width), bf16),
        ((A, count, width), bf16),
        ((A - 1, count, width), bf16),
        ((A - 1, count, width), bf16),
    ]
    return pl.pallas_call(
        functools.partial(layer_kernel, n),
        out_shape=jax.ShapeDtypeStruct((count, width), bf16),
        in_specs=[vmem] * 5 + [smem] + [vmem] + [hbm] * 9,
        out_specs=vmem,
        scratch_shapes=[pltpu.VMEM(s, t) for s, t in scratch]
        + [
            pltpu.SemaphoreType.DMA((7,)),
            pltpu.SemaphoreType.DMA((count,)),
            pltpu.SemaphoreType.DMA((count,)),
            pltpu.SemaphoreType.DMA((7, n - 1)),
            pltpu.SemaphoreType.DMA((7, n - 1)),
        ],
        compiler_params=pltpu.CompilerParams(
            collective_id=0, has_side_effects=True, vmem_limit_bytes=62 * 1024 * 1024
        ),
        name="layer",
    )(
        tokens,
        norm_gain.reshape(1, width),
        head_gain.reshape(1, val),
        moe_gain.reshape(1, width),
        lambdas.reshape(heads, 1),
        lengths,
        shares,
        query_weight,
        key_weight,
        value_weight,
        out_weight,
        cache_keys.reshape(count, ctx2, lanes),
        cache_values.reshape(count, ctx2, val),
        gate_weight,
        up_weight,
        down_weight,
    )


def solution(mesh):
    placed = (
        P(("grp", "ep"), None),
        P(),
        P(None, "ep"),
        P(),
        P(),
        P(None, "ep"),
        P(),
        P(),
        P(("grp", "ep"), None, None, None),
        P(("grp", "ep"), None, None, None),
        P(("grp", "ep")),
        P(),
        P("ep", None, None),
        P("ep", None, None),
        P("ep", None, None),
        P(("grp", "ep"), None),
        P(("grp", "ep"), None),
    )
    return jax.shard_map(
        functools.partial(local, mesh.shape["ep"]),
        mesh=mesh,
        in_specs=placed,
        out_specs=P(("grp", "ep"), None),
        check_vma=False,
    )
```

time: 171 us -> 89.4 us (0.52)
  waiting for transfers between devices: 82.1 us -> 0 us
  Pallas kernels: 0 us -> 80.5 us
  matrix products: 24.5 us -> 0 us
  blocking collectives: 17 us -> 0 us
  local copies, waits for them, and re-layouts: 23.9 us -> 7.9 us
  between operations: 13.6 us -> 0.01 us
  starting transfers between devices: 4.2 us -> 0 us
  other arithmetic: 4.52 us -> 0.71 us
    pallas_call x0 -> x1, Pallas kernels: none -> 80.5 us  [local(): pl.pallas_call(functools.partial(layer_kernel, n), out_shape=jax.ShapeDty...]
    all_gather x2 -> x0, waiting for transfers between devices: 66.6 us -> none  [the longest x1 37.6 us: local(): lax.all_gather(out_weight, 'ep', axis=1, tiled=True)]
    dot_general x10 -> x0, matrix products: 24.5 us -> none  [the longest x1 5.7 us: expert_mlp(): jnp.dot(act, down_w, preferred_element_type=jnp.float32)]
    unnamed x23 -> x2, local copies, waits for them, and re-layouts: 21.5 us -> 3.42 us
    all_to_all x1 -> x0, blocking collectives: 17 us -> none  [local(): lax.all_to_all(outgoing, 'ep', split_axis=0, concat_axis=0, tiled=True)]
    all_to_all x1 -> x0, waiting for transfers between devices: 14.1 us -> none  [local(): lax.all_to_all(results, 'ep', split_axis=0, concat_axis=0, tiled=True)]
    all_to_all x1 -> x0, starting transfers between devices: 4.16 us -> none  [local(): lax.all_to_all(results, 'ep', split_axis=0, concat_axis=0, tiled=True)]
    reshape x3, local copies, waits for them, and re-layouts: 0.3 us -> 3.88 us  [the longest x1 1.31 us: local(): lambdas.reshape(heads, 1)]
  transfers between devices with their start and end apart: 3 -> 0, of which waited for: 3 -> 0; matrix products, arithmetic and copies ran while one was open for 24% -> 0% of each run, Pallas kernels for 0% -> 0%
where the time goes in v1:
time: 89.4 us; the launch traced here: 89.1 us
  Pallas kernels  80.5 us (90%)
  local copies, waits for them, and re-layouts  7.9 us (9%)
    pallas_call x1, Pallas kernels, local(): pl.pallas_call(functools.partial(layer_kernel, n), out_shape=jax.ShapeDty...  80.5 us
    unnamed x2, local copies, waits for them, and re-layouts  3.42 us

profile of v1, /device:TPU:0, one launch (start us, length us, event | category | flops | bytes accessed | tf_op | source)
XLA Modules:
  0.0 89.1 jit_solution(4089438544457151242)
XLA Ops:
  0.0 1.3 %copy.22.lambdas_ref = f32[8,1]{1,0:T(8,128)} copy(f32[8,1]{0,1:T(1,128)} %bitcast.8) | data formatting | bytes 64 | tf_op jit(solution)/shard_map/reshape | solution.py:481
  1.3 1.3 %reshape.20.norm_gain_ref = bf16[1,2048]{1,0:T(2,128)(2,1)} reshape(bf16[2048]{0:T(1024)(128)(2,1)} %param.18) | data formatting | bytes 8192 | tf_op jit(solution)/shard_map/reshape | solution.py:478
  2.6 1.3 %reshape.22.moe_gain_ref = bf16[1,2048]{1,0:T(2,128)(2,1)} reshape(bf16[2048]{0:T(1024)(128)(2,1)} %param.28) | data formatting | bytes 8192 | tf_op jit(solution)/shard_map/reshape | solution.py:480
  3.9 0.7 select_reduce_fusion
  4.6 0.6 pad.4
  5.2 1.9 %copy.23.wq_hbm = bf16[2048,64]{1,0:T(8,128)(2,1)} copy(bf16[2048,64]{0,1:T(8,128)(2,1)} %param.19) | data formatting | bytes 524288 | tf_op args[2]
  7.1 80.5 %layer.1 = bf16[16,2048]{1,0:T(8,128)(2,1)} custom-call(bf16[16,2048]{1,0:T(8,128)(2,1)} %tokens_ref.1, bf16[1,2048]{1,0:T(2,128)(2,1)} %reshape.20.norm_gain_ref, bf16[1,128]{1,0:T(2,128)(2,1)} %bitcast.9, bf16[1,2048]{1,0:T(2,128)(2,1)} %reshape.22.moe_gain_ref, f32[8,1]{1,0:T(8,128)} %copy.22.lambdas_ref, s32[16]{0:T(128)} %lengths_ref.1, ...), custom_call_target="tpu_custom_call" | custom-call | tf_op jit(solution)/shard_map/layer/pallas_call | solution.py:459
  87.6 1.5 %copy.25 = bf16[16,2048]{1,0:T(8,128)(2,1)} copy(bf16[16,2048]{1,0:T(8,128)(2,1)} %layer.1) | data formatting | bytes 131072

commit v2 on v1

v2 whole, which is shorter than its diff:
```python
import functools

import jax
import jax.numpy as jnp
from jax import lax
from jax.experimental import pallas as pl
from jax.experimental.pallas import tpu as pltpu
from jax.sharding import PartitionSpec as P

epsilon = 1e-06
masked_score = -1e30
clamp_limit = 7.0
swish_alpha = 1.702
f32 = jnp.float32
bf16 = jnp.bfloat16


def rms_scaled(values, gain):
    floats = values.astype(f32)
    scale = lax.rsqrt(jnp.mean(floats * floats, axis=-1, keepdims=True) + epsilon)
    return floats * scale * gain.astype(f32)


def layer_kernel(
    n,
    tokens_ref,
    norm_gain_ref,
    head_gain_ref,
    moe_gain_ref,
    lambdas_ref,
    lengths_ref,
    routes_ref,
    route_weights_ref,
    wq_hbm,
    wk_hbm,
    wv_hbm,
    wo_hbm,
    keys_hbm,
    values_hbm,
    gate_hbm,
    up_hbm,
    down_hbm,
    out_ref,
    wq,
    wk,
    wv,
    wo,
    keys,
    values,
    gate_w,
    up_w,
    down_w,
    normed_all,
    heads_all,
    moe_all,
    q_out,
    q_in,
    ao_out,
    ao_in,
    shares_out,
    shares_in,
    share,
    q_grid,
    own_k,
    own_v,
    ho_grid,
    residual,
    act,
    y_out,
    rs_sib,
    rs_y_send,
    rs_y,
    rs_z_send,
    rs_z,
    w_sem,
    k_sem,
    v_sem,
    send_sem,
    recv_sem,
):
    me = lax.axis_index("ep")
    A = n // 4
    a, b, c = me // 4, (me // 2) % 2, me % 2
    count, width = tokens_ref.shape
    heads = lambdas_ref.shape[0]
    ctx2, lanes = keys.shape[1], keys.shape[2]
    kv_count = wk.shape[1] // lanes
    group = heads // kv_count
    dh = lanes // 2
    val = values.shape[2]

    def idx(i, j, k):
        return (i * 2 + j) * 2 + k

    def fwd(d):
        return lax.rem(a + d, A)

    def back(d):
        return lax.rem(a - d + A, A)

    ydev, sdev = idx(a, 1 - b, c), idx(a, b, 1 - c)
    sent = []

    def remote(src, dst, k, j, dev):
        return pltpu.make_async_remote_copy(
            src_ref=src,
            dst_ref=dst,
            send_sem=send_sem.at[k, j],
            recv_sem=recv_sem.at[k, j],
            device_id={"ep": dev},
            device_id_type=pl.DeviceIdType.MESH,
        )

    def start(copy):
        copy.start()
        sent.append(copy)

    loads = [
        pltpu.make_async_copy(src, dst, w_sem.at[i])
        for i, (src, dst) in enumerate(
            [
                (wq_hbm, wq.at[b * 2 + c]),
                (wk_hbm, wk),
                (wv_hbm, wv),
                (wo_hbm, wo.at[b * 2 + c]),
                (gate_hbm.at[0], gate_w),
                (up_hbm.at[0], up_w),
                (down_hbm.at[0], down_w),
            ]
        )
    ]

    def key_load(s):
        return pltpu.make_async_copy(keys_hbm.at[s], keys.at[s], k_sem.at[s])

    def value_load(s):
        return pltpu.make_async_copy(values_hbm.at[s], values.at[s], v_sem.at[s])

    barrier = pltpu.get_barrier_semaphore()

    def greet(d, carry):
        pl.semaphore_signal(
            barrier,
            inc=1,
            device_id={"ep": lax.rem(me + d, n)},
            device_id_type=pl.DeviceIdType.MESH,
        )
        return carry

    lax.fori_loop(1, n, greet, 0)
    for i in (0, 3, 1, 2):
        loads[i].start()

    def cache_load(s, carry):
        key_load(s).start()
        value_load(s).start()
        return carry

    lax.fori_loop(0, count, cache_load, 0)
    for i in range(4, 7):
        loads[i].start()

    normed_all[a] = rms_scaled(
        tokens_ref[...], norm_gain_ref[...].reshape(1, width)
    ).astype(bf16)
    topk = routes_ref.shape[0]
    expert = lax.broadcasted_iota(jnp.int32, (n, count), 0)
    routed = jnp.zeros((n, count), f32)
    for k in range(topk):
        routed = routed + jnp.where(
            routes_ref[k : k + 1, :] == expert, route_weights_ref[k : k + 1, :], 0.0
        )
    shares_out[...] = jnp.zeros_like(shares_out)
    shares_out[:, 0, :count] = routed
    pl.semaphore_wait(barrier, n - 1)

    def share_weight(buf, k):
        own = b * 2 + c
        start(remote(buf.at[own], buf.at[own], k, 0, ydev))
        start(remote(buf.at[own], buf.at[own], k, 1, sdev))

    def share_weight_on(buf, k):
        other = (1 - b) * 2 + c
        remote(buf.at[other], buf.at[other], k, 0, ydev).wait_recv()
        start(remote(buf.at[other], buf.at[other], k, 2, sdev))

    def share_weight_wait(buf, k):
        for j in range(2):
            slot = lax.rem(b + j, 2) * 2 + 1 - c
            remote(buf.at[slot], buf.at[slot], k, 1 + j, sdev).wait_recv()

    def line_start(src, dst, k, same):
        for d in range(1, A):
            dev = idx(fwd(d), b, c)
            start(remote(src.at[a if same else fwd(d)], dst.at[a], k, d - 1, dev))

    def line_wait(dst, k):
        for d in range(1, A):
            slot = back(d)
            remote(dst.at[slot], dst.at[slot], k, d - 1, idx(slot, b, c)).wait_recv()

    def place(i, j, k):
        return (j * A + i) * 2 + k

    def exchange_start(src, dst, k):
        def body(d, carry):
            peer = lax.rem(me + d, n)
            remote(src.at[peer], dst.at[me], k, d - 1, peer).start()
            return carry

        lax.fori_loop(1, n, body, 0)

    def exchange_wait(src, dst, k):
        def body(d, carry):
            peer = lax.rem(me - d + n, n)
            remote(src.at[peer], dst.at[peer], k, d - 1, peer).wait_recv()
            return carry

        lax.fori_loop(1, n, body, 0)

    def exchange_drain(src, dst, k):
        def body(d, carry):
            peer = lax.rem(me + d, n)
            remote(src.at[peer], dst.at[me], k, d - 1, peer).wait_send()
            return carry

        lax.fori_loop(1, n, body, 0)

    line_start(normed_all, normed_all, 0, True)
    loads[0].wait()
    share_weight(wq, 7)
    loads[3].wait()
    share_weight(wo, 8)
    exchange_start(shares_out, shares_in, 6)
    shares_in[me] = shares_out[me]
    loads[1].wait()
    loads[2].wait()
    mine = normed_all[a]
    own_k[:, 0, :] = jnp.dot(mine, wk[...], preferred_element_type=f32).astype(bf16).astype(f32)
    own_v[:, 0, :] = jnp.dot(mine, wv[...], preferred_element_type=f32).astype(bf16).astype(f32)
    share_weight_on(wq, 7)
    line_wait(normed_all, 0)
    share_weight_wait(wq, 7)
    qw = wq.shape[1]
    q = lax.dot_general(
        normed_all[...].reshape(A * count, width),
        wq[...].reshape(4 * qw, width),
        (((1,), (1,)), ((), ())),
        preferred_element_type=f32,
    )
    q_out[...] = q.astype(bf16).reshape(A, count, 4 * qw)
    line_start(q_out, q_in, 3, False)
    q_in[a] = q_out[a]
    share_weight_on(wo, 8)
    line_wait(q_in, 3)
    per_block = 4 * qw // lanes
    lane_map = lax.broadcasted_iota(jnp.int32, (count, lanes), 1) // dh
    for h in range(heads):
        first = (h % per_block) * lanes
        both = q_in[h // per_block, :, first : first + lanes].astype(f32)
        for m in range(2):
            q_grid[:, m * heads + h, :] = jnp.where(lane_map == m, both, 0.0)

    inv_scale = dh ** (-0.5)
    rows = 2 * heads
    kv_of = lax.rem(lax.broadcasted_iota(jnp.int32, (rows, ctx2), 0), heads) // group
    column = lax.broadcasted_iota(jnp.int32, (rows, ctx2), 1)
    head_row = lax.broadcasted_iota(jnp.int32, (heads, 1), 0)
    lam = jnp.zeros((heads, 1), f32)
    for h in range(heads):
        lam = jnp.where(head_row == h, lambdas_ref[h], lam)
    matched = lax.rem(column, kv_count) == kv_of
    row_kv = lax.rem(lax.broadcasted_iota(jnp.int32, (rows, lanes), 0), heads) // group
    head_gain = head_gain_ref[...].astype(f32)
    step = 4 if count % 4 == 0 else 1

    def attend(i, carry):
        seqs = [i * step + u for u in range(step)]
        for s in seqs:
            key_load(s).wait()
            value_load(s).wait()
        queries = [q_grid[s] for s in seqs]
        scores = [
            lax.dot_general(
                qs.astype(bf16),
                keys[s],
                (((1,), (1,)), ((), ())),
                preferred_element_type=f32,
            )
            * inv_scale
            for s, qs in zip(seqs, queries)
        ]
        weights, own_parts = [], []
        for s, qs, score in zip(seqs, queries, scores):
            own_key = jnp.zeros((rows, lanes), f32)
            own_val = jnp.zeros((heads, val), f32)
            for kv in range(kv_count):
                own_key = jnp.where(
                    row_kv == kv, own_k[s, :, kv * lanes : (kv + 1) * lanes], own_key
                )
                own_val = jnp.where(
                    row_kv[:heads] == kv, own_v[s, :, kv * val : (kv + 1) * val], own_val
                )
            own_score = jnp.sum(qs * own_key, axis=1, keepdims=True) * inv_scale
            visible = matched & (column < lengths_ref[s] * kv_count)
            score = jnp.where(visible, score, masked_score)
            highest = jnp.maximum(jnp.max(score, axis=1, keepdims=True), own_score)
            expd = jnp.exp(score - highest)
            own_exp = jnp.exp(own_score - highest)
            inv = 1.0 / (jnp.sum(expd, axis=1, keepdims=True) + own_exp)
            own_prob = own_exp * inv
            weights.append(
                (expd[:heads] * inv[:heads] - expd[heads:] * (lam * inv[heads:])).astype(bf16)
            )
            own_weight = (own_prob[:heads] - lam * own_prob[heads:]).astype(bf16).astype(f32)
            own_parts.append(own_weight * own_val)
        sums = [
            jnp.dot(w, values[s], preferred_element_type=f32) for s, w in zip(seqs, weights)
        ]
        for s, attended, own in zip(seqs, sums, own_parts):
            ho_grid[s] = rms_scaled(attended + own, head_gain)
        return carry

    lax.fori_loop(0, count // step, attend, 0)
    for h in range(heads):
        heads_all[a, :, h * val : (h + 1) * val] = ho_grid[:, h, :].astype(bf16)

    line_start(heads_all, heads_all, 1, True)
    share_weight_wait(wo, 8)
    line_wait(heads_all, 1)
    ow = wo.shape[2]
    head_rows = heads_all[...].reshape(A * count, heads * val)
    ao = jnp.concatenate(
        [jnp.dot(head_rows, wo[j], preferred_element_type=f32) for j in range(4)], axis=1
    )
    ao_out[...] = ao.astype(bf16).reshape(A, count, 4 * ow)
    line_start(ao_out, ao_in, 4, False)
    ao_in[a] = ao_out[a]
    line_wait(ao_in, 4)
    for t in range(A):
        cols = slice(t * 4 * ow, (t + 1) * 4 * ow)
        residual[:, cols] = (
            (tokens_ref[:, cols].astype(f32) + ao_in[t].astype(f32)).astype(bf16).astype(f32)
        )

    mine_at = place(a, b, c)
    moe_all[mine_at] = rms_scaled(residual[...], moe_gain_ref[...].reshape(1, width)).astype(bf16)

    def cp(slot, j, dev):
        return remote(moe_all.at[slot], moe_all.at[slot], 2, j, dev)

    for d in range(1, A):
        start(cp(mine_at, d - 1, idx(fwd(d), b, c)))
    start(cp(mine_at, A - 1, ydev))
    start(cp(mine_at, 2 * A - 1, sdev))
    for d in range(1, A):
        slot = place(back(d), b, c)
        cp(slot, d - 1, me).wait_recv()
        start(cp(slot, A - 1 + d, ydev))
        start(cp(slot, 2 * A - 1 + d, sdev))
    for i in range(4, 7):
        loads[i].wait()
    for d in range(A):
        cp(place(back(d), b, 1 - c), 2 * A - 1 + d, me).wait_recv()
    half = 2 * A
    half_rows = half * count
    ff = gate_w.shape[1]
    tile = 256

    def hidden(which):
        def body(i, carry):
            cols = pl.ds(pl.multiple_of(i * tile, tile), tile)
            x = moe_all[pl.ds(which * half, half)].reshape(half_rows, width)
            gate = jnp.dot(x, gate_w[:, cols], preferred_element_type=f32)
            upper = jnp.dot(x, up_w[:, cols], preferred_element_type=f32)
            gate = jnp.minimum(gate, clamp_limit)
            upper = jnp.clip(upper, -clamp_limit, clamp_limit)
            value = (upper + 1.0) * gate * jax.nn.sigmoid(swish_alpha * gate)
            act[which, :, cols] = value.astype(bf16)
            return carry

        lax.fori_loop(0, ff // tile, body, 0)

    hidden(b)
    for d in range(A):
        slot = place(back(d), 1 - b, c)
        cp(slot, A - 1 + d, me).wait_recv()
        start(cp(slot, 3 * A - 1 + d, sdev))
    exchange_wait(shares_out, shares_in, 6)
    diagonal = lax.broadcasted_iota(jnp.int32, (count, lanes), 0) == lax.broadcasted_iota(
        jnp.int32, (count, lanes), 1
    )
    for i in range(A):
        for j in range(2):
            for k in range(2):
                row = shares_in[idx(i, j, k)]
                share[place(i, j, k)] = jnp.sum(
                    jnp.where(diagonal, row, 0.0), axis=1, keepdims=True
                )
    for d in range(A):
        cp(place(back(d), 1 - b, 1 - c), 3 * A - 1 + d, me).wait_recv()
    hidden(1 - b)

    def project(which):
        part = share[pl.ds(which * half, half)].reshape(half_rows, 1)

        def body(i, carry):
            cols = pl.ds(pl.multiple_of(i * tile, tile), tile)
            y = jnp.dot(act[which], down_w[:, cols], preferred_element_type=f32)
            y_out[pl.ds(which * half, half), :, cols] = (
                (y * part).astype(bf16).reshape(half, count, tile)
            )
            return carry

        lax.fori_loop(0, width // tile, body, 0)

    order = list(range(1, A)) + [0]

    def sib(d, j):
        return remote(
            y_out.at[place(fwd(d), lax.rem(b + j, 2), 1 - c)],
            rs_sib.at[fwd(d) * 2 + lax.rem(b + j, 2)],
            5,
            2 * A - 1 + j * A + d,
            sdev,
        )

    for j in (1, 0):
        project(lax.rem(b + j, 2))
        for d in order:
            start(sib(d, j))
    ycopies, zcopies = {}, {}
    for d in order:
        sib(d, 1).wait_recv()
        dest = fwd(d)
        rs_y_send[d] = (
            y_out[place(dest, 1 - b, c)].astype(f32) + rs_sib[dest * 2 + 1 - b].astype(f32)
        ).astype(bf16)
        ycopies[d] = remote(rs_y_send.at[d], rs_y.at[d], 5, A - 1 + d, ydev)
        start(ycopies[d])
    total = residual[...]
    for d in order:
        sib(d, 0).wait_recv()
        ycopies[d].wait_recv()
        dest = fwd(d)
        part = (
            y_out[place(dest, b, c)].astype(f32)
            + rs_sib[dest * 2 + b].astype(f32)
            + rs_y[d].astype(f32)
        )
        if d:
            rs_z_send[d - 1] = part.astype(bf16)
            zcopies[d] = remote(
                rs_z_send.at[d - 1], rs_z.at[d - 1], 5, d - 1, idx(dest, b, c)
            )
            start(zcopies[d])
        else:
            total = total + part
    for d in range(1, A):
        zcopies[d].wait_recv()
        total = total + rs_z[d - 1].astype(f32)
    out_ref[...] = total.astype(bf16)
    for copy in sent:
        copy.wait_send()
    exchange_drain(shares_out, shares_in, 6)


def local(
    n,
    tokens,
    norm_gain,
    query_weight,
    key_weight,
    value_weight,
    out_weight,
    head_gain,
    lambdas,
    cache_keys,
    cache_values,
    lengths,
    moe_gain,
    gate_weight,
    up_weight,
    down_weight,
    routes,
    route_weights,
):
    count, width = tokens.shape
    heads = lambdas.shape[0]
    ctx, kv_count, lanes = cache_keys.shape[1:]
    val = cache_values.shape[3]
    ctx2 = ctx * kv_count
    ff = gate_weight.shape[2]
    A = n // 4
    vmem = pl.BlockSpec(memory_space=pltpu.VMEM)
    smem = pl.BlockSpec(memory_space=pltpu.SMEM)
    hbm = pl.BlockSpec(memory_space=pl.ANY)
    scratch = [
        ((4,) + query_weight.shape[::-1], bf16),
        (key_weight.shape, bf16),
        (value_weight.shape, bf16),
        ((4,) + out_weight.shape, bf16),
        ((count, ctx2, lanes), bf16),
        ((count, ctx2, val), bf16),
        ((width, ff), bf16),
        ((width, ff), bf16),
        ((ff, width), bf16),
        ((A, count, width), bf16),
        ((A, count, heads * val), bf16),
        ((n, count, width), bf16),
        ((A, count, 4 * query_weight.shape[1]), bf16),
        ((A, count, 4 * query_weight.shape[1]), bf16),
        ((A, count, 4 * out_weight.shape[1]), bf16),
        ((A, count, 4 * out_weight.shape[1]), bf16),
        ((n, 1, lanes), f32),
        ((n, 1, lanes), f32),
        ((n, count, 1), f32),
        ((count, 2 * heads, lanes), f32),
        ((count, 1, kv_count * lanes), f32),
        ((count, 1, kv_count * val), f32),
        ((count, heads, val), f32),
        ((count, width), f32),
        ((2, n * count // 2, ff), bf16),
        ((n, count, width), bf16),
        ((2 * A, count, width), bf16),
        ((A, count, width), bf16),
        ((A, count, width), bf16),
        ((A - 1, count, width), bf16),
        ((A - 1, count, width), bf16),
    ]
    return pl.pallas_call(
        functools.partial(layer_kernel, n),
        out_shape=jax.ShapeDtypeStruct((count, width), bf16),
        in_specs=[vmem] * 4 + [smem] * 2 + [vmem] * 2 + [hbm] * 9,
        out_specs=vmem,
        scratch_shapes=[pltpu.VMEM(s, t) for s, t in scratch]
        + [
            pltpu.SemaphoreType.DMA((7,)),
            pltpu.SemaphoreType.DMA((count,)),
            pltpu.SemaphoreType.DMA((count,)),
            pltpu.SemaphoreType.DMA((9, n - 1)),
            pltpu.SemaphoreType.DMA((9, n - 1)),
        ],
        compiler_params=pltpu.CompilerParams(
            collective_id=0, has_side_effects=True, vmem_limit_bytes=62 * 1024 * 1024
        ),
        name="layer",
    )(
        tokens,
        norm_gain,
        head_gain.reshape(1, val),
        moe_gain,
        lambdas,
        lengths,
        routes.T,
        route_weights.T,
        query_weight.T,
        key_weight,
        value_weight,
        out_weight,
        cache_keys.reshape(count, ctx2, lanes),
        cache_values.reshape(count, ctx2, val),
        gate_weight,
        up_weight,
        down_weight,
    )


def solution(mesh):
    placed = (
        P(("grp", "ep"), None),
        P(),
        P(None, "ep"),
        P(),
        P(),
        P(None, "ep"),
        P(),
        P(),
        P(("grp", "ep"), None, None, None),
        P(("grp", "ep"), None, None, None),
        P(("grp", "ep")),
        P(),
        P("ep", None, None),
        P("ep", None, None),
        P("ep", None, None),
        P(("grp", "ep"), None),
        P(("grp", "ep"), None),
    )
    return jax.shard_map(
        functools.partial(local, mesh.shape["ep"]),
        mesh=mesh,
        in_specs=placed,
        out_specs=P(("grp", "ep"), None),
        check_vma=False,
    )
```

time: 89.4 us -> 65.4 us (0.73)
  Pallas kernels: 80.5 us -> 63.8 us
  local copies, waits for them, and re-layouts: 7.9 us -> 1.47 us
    pallas_call x1, Pallas kernels: 80.5 us -> 63.8 us  [local(): pl.pallas_call(functools.partial(layer_kernel, n), out_shape=jax.ShapeDty...]
    reshape x3 -> x0, local copies, waits for them, and re-layouts: 3.88 us -> none  [the longest x1 1.31 us: local(): lambdas.reshape(heads, 1)]
    unnamed x2 -> x1, local copies, waits for them, and re-layouts: 3.42 us -> 1.47 us
where the time goes in v2:
time: 65.4 us; the launch traced here: 65.2 us
  Pallas kernels  63.8 us (98%)
  local copies, waits for them, and re-layouts  1.47 us (2%)
    pallas_call x1, Pallas kernels, local(): pl.pallas_call(functools.partial(layer_kernel, n), out_shape=jax.ShapeDty...  63.8 us
    unnamed x1, local copies, waits for them, and re-layouts  1.47 us

profile of v2, /device:TPU:0, one launch (start us, length us, event | category | flops | bytes accessed | tf_op | source)
XLA Modules:
  0.0 65.2 jit_solution(14208009300565225599)
XLA Ops:
  0.0 63.8 %layer.1 = bf16[16,2048]{1,0:T(8,128)(2,1)} custom-call(bf16[16,2048]{1,0:T(8,128)(2,1)} %tokens_ref.1, bf16[2048]{0:T(1024)(128)(2,1)} %norm_gain_ref.1, bf16[1,128]{1,0:T(2,128)(2,1)} %bitcast.11, bf16[2048]{0:T(1024)(128)(2,1)} %moe_gain_ref.1, f32[8]{0:T(128)} %lambdas_ref.1, s32[16]{0:T(128)} %lengths_ref.1, s32[4,16]{1,0:T(4,128)} %bitcast.9, ...), custom_call_target="tpu_custom_call" | custom-call | tf_op jit(solution)/shard_map/layer/pallas_call | solution.py:531
  63.8 1.5 %copy.19 = bf16[16,2048]{1,0:T(8,128)(2,1)} copy(bf16[16,2048]{1,0:T(8,128)(2,1)} %layer.1) | data formatting | bytes 131072

commit v3 on v2

--- a/solution.py
+++ b/solution.py
@@ -397,10 +397,6 @@
                 share[place(i, j, k)] = jnp.sum(
                     jnp.where(diagonal, row, 0.0), axis=1, keepdims=True
                 )
-    for d in range(A):
-        cp(place(back(d), 1 - b, 1 - c), 3 * A - 1 + d, me).wait_recv()
-    hidden(1 - b)
-
     def project(which):
         part = share[pl.ds(which * half, half)].reshape(half_rows, 1)
 
@@ -425,10 +421,15 @@
             sdev,
         )
 
-    for j in (1, 0):
-        project(lax.rem(b + j, 2))
-        for d in order:
-            start(sib(d, j))
+    project(b)
+    for d in order:
+        start(sib(d, 0))
+    for d in range(A):
+        cp(place(back(d), 1 - b, 1 - c), 3 * A - 1 + d, me).wait_recv()
+    hidden(1 - b)
+    project(1 - b)
+    for d in order:
+        start(sib(d, 1))
     ycopies, zcopies = {}, {}
     for d in order:
         sib(d, 1).wait_recv()

time: 65.4 us -> 65.8 us (level)
  no operation moved by 1% of the time
where the time goes in v3:
time: 65.8 us; the launch traced here: 65.6 us
  Pallas kernels  64.1 us (97%)
  local copies, waits for them, and re-layouts  1.47 us (2%)
    pallas_call x1, Pallas kernels, local(): pl.pallas_call(functools.partial(layer_kernel, n), out_shape=jax.ShapeDty...  64.1 us
    unnamed x1, local copies, waits for them, and re-layouts  1.47 us

profile of v3, /device:TPU:0, one launch (start us, length us, event | category | flops | bytes accessed | tf_op | source)
XLA Modules:
  0.0 65.6 jit_solution(16359760675899773126)
XLA Ops:
  0.0 64.1 %layer.1 = bf16[16,2048]{1,0:T(8,128)(2,1)} custom-call(bf16[16,2048]{1,0:T(8,128)(2,1)} %tokens_ref.1, bf16[2048]{0:T(1024)(128)(2,1)} %norm_gain_ref.1, bf16[1,128]{1,0:T(2,128)(2,1)} %bitcast.11, bf16[2048]{0:T(1024)(128)(2,1)} %moe_gain_ref.1, f32[8]{0:T(128)} %lambdas_ref.1, s32[16]{0:T(128)} %lengths_ref.1, s32[4,16]{1,0:T(4,128)} %bitcast.9, ...), custom_call_target="tpu_custom_call" | custom-call | tf_op jit(solution)/shard_map/layer/pallas_call | solution.py:532
  64.1 1.5 %copy.19 = bf16[16,2048]{1,0:T(8,128)(2,1)} copy(bf16[16,2048]{1,0:T(8,128)(2,1)} %layer.1) | data formatting | bytes 131072
